TPU v7x, 32 devices: a whole 2x2x4 slice. The times are simulated.
32 devices in a mesh: sp: 8 (over z, y), tp: 4 (over x, core).
Axes of the slice: x: 2, y: 2, z: 4, core: 2. Of those that a mesh axis runs over, the one named last changes fastest.
Arguments:
- queries: bfloat16 [6144, 2048], P('sp', 'tp'), may hold values from -11 to 11
- key_rows: bfloat16 [6144, 2048], P('sp', 'tp'), may hold values from -4.5 to 4.5
- value_rows: bfloat16 [6144, 2048], P('sp', 'tp'), may hold values from -6 to 6
- log_forget: float32 [6144, 32], P('sp', 'tp'), may hold values from -740.28 to 0, as said below
- stream_in: bfloat16 [6144, 2048], P('sp'), may hold values from -6 to 6
- out_weight: bfloat16 [2048, 2048], P('tp'), may hold values from -0.52734375 to 0.52734375
- mix_gain: float32 [2048], replicated, may hold values from 0.1 to 1.9
- mix_bias: float32 [2048], replicated, may hold values from -3 to 3
- gate_weight: bfloat16 [2048, 5632], P('sp', 'tp'), may hold values from -0.125 to 0.125
- up_weight: bfloat16 [2048, 5632], P('sp', 'tp'), may hold values from -0.125 to 0.125
- down_weight: bfloat16 [5632, 2048], P('tp', 'sp'), may hold values from -0.15917969 to 0.15917969
- ffn_gain: float32 [2048], replicated, may hold values from 0.1 to 1.9
- ffn_bias: float32 [2048], replicated, may hold values from -3 to 3
Outputs:
- layer_out: bfloat16 [6144, 2048], P(('sp', 'tp'))
Inputs may be any that keep to these rules, and one draw needn't show every extreme that they name: `log_forget`: each column never rises along the positions.
All inputs are finite; a program needn't handle non-finite values.
Results may differ from a plain program's by a relative error of at most 0.015.
Values may be sent and summed in bfloat16 or wider, within the bound.
A program may use at most 128 MiB of HBM per device.

v0:
```python
import jax
import jax.numpy as jnp
from jax import lax
from jax.sharding import PartitionSpec as P

ALPHA = 8.0**0.25
EPSILON = 1e-05


def layer_norm(matrix, norm_gain, norm_shift):
    centred = matrix - jnp.mean(matrix, axis=-1, keepdims=True)
    spread = jnp.mean(centred * centred, axis=-1, keepdims=True)
    return centred * lax.rsqrt(spread + EPSILON) * norm_gain + norm_shift


def attend(queries, key_rows, value_rows, log_forget):
    length, row_width = queries.shape
    head_count = log_forget.shape[1]
    head_dim = row_width // head_count
    score_scale = head_dim ** (-0.5)
    first_pos = lax.axis_index("sp") * length
    last_pos = first_pos + length
    query_heads = queries.reshape(length, head_count, head_dim)
    query_gates = log_forget.T
    query_pos = first_pos + jnp.arange(length, dtype=jnp.int32)
    gates_all = lax.all_gather(log_forget, "sp", axis=0, tiled=True)
    initial = (
        jnp.full((head_count, length), -1e30, jnp.float32),
        jnp.zeros((head_count, length), jnp.float32),
        jnp.zeros((length, head_count, head_dim), jnp.float32),
    )
    running = initial
    key_piece = lax.all_gather(key_rows, "sp", axis=0, tiled=True)
    value_piece = lax.all_gather(value_rows, "sp", axis=0, tiled=True)
    piece_len = key_piece.shape[0]
    shards = piece_len // length
    group_size = max(
        [
            count_try
            for count_try in range(1, shards + 1)
            if shards % count_try == 0 and count_try * length <= max(length, 512)
        ]
    )
    block_len = group_size * length
    blocks = piece_len // block_len
    key_blocks = key_piece.reshape(blocks, block_len, head_count, head_dim)
    value_blocks = value_piece.reshape(blocks, block_len, head_count, head_dim)
    gate_blocks = gates_all.reshape(blocks, block_len, head_count)
    block_starts = block_len * jnp.arange(blocks, dtype=jnp.int32)

    def one_block(running_state, packed):
        key_block, value_block, gate_block, block_start = packed

        def compute(state_in):
            highest, totals, weighted = state_in
            scores = (
                jnp.einsum(
                    "qhd,khd->hqk", query_heads, key_block, preferred_element_type=jnp.float32
                )
                * score_scale
            )
            scores = scores + query_gates[:, :, None] - gate_block.T[:, None, :]
            key_pos = block_start + jnp.arange(block_len, dtype=jnp.int32)
            allowed = (key_pos[None, :] <= query_pos[:, None])[None]
            masked = jnp.where(allowed, scores, -1e30)
            new_high = jnp.maximum(highest, jnp.max(masked, axis=2))
            weights = jnp.where(allowed, jnp.exp(masked - new_high[:, :, None]), 0.0)
            factor = jnp.exp(highest - new_high)
            totals = totals * factor + jnp.sum(weights, axis=2)
            weighted = weighted * factor.T[:, :, None] + jnp.einsum(
                "hqk,khd->qhd",
                weights.astype(jnp.bfloat16),
                value_block,
                preferred_element_type=jnp.float32,
            )
            return (new_high, totals, weighted)

        def keep_state(state_in):
            return state_in

        return (lax.cond(block_start < last_pos, compute, keep_state, running_state), None)

    running, unused = lax.scan(
        one_block, running, (key_blocks, value_blocks, gate_blocks, block_starts)
    )
    highest, totals, weighted = running
    return (weighted / totals.T[:, :, None]).reshape(length, row_width).astype(jnp.bfloat16)


def body(
    queries,
    key_rows,
    value_rows,
    log_forget,
    stream_in,
    out_weight,
    mix_gain,
    mix_bias,
    gate_weight,
    up_weight,
    down_weight,
    ffn_gain,
    ffn_bias,
):
    attended = attend(queries, key_rows, value_rows, log_forget)
    length = attended.shape[0]
    own_rows = length // lax.axis_size("tp")
    offset = lax.axis_index("tp") * own_rows
    summed = lax.psum_scatter(
        jnp.dot(attended, out_weight, preferred_element_type=jnp.float32).astype(jnp.bfloat16),
        "tp",
        scatter_dimension=0,
        tiled=True,
    )
    mix_out = lax.optimization_barrier(summed).astype(jnp.float32)
    stream_own = lax.dynamic_slice_in_dim(stream_in, offset, own_rows, 0)
    normed = layer_norm(
        ALPHA * stream_own.astype(jnp.float32) + mix_out, mix_gain, mix_bias
    ).astype(jnp.bfloat16)
    gathered = lax.all_gather(normed, "tp", axis=0, tiled=True)
    gate_part = jnp.dot(
        gathered,
        lax.all_gather(gate_weight, "sp", axis=0, tiled=True),
        preferred_element_type=jnp.float32,
    )
    up_part = jnp.dot(
        gathered,
        lax.all_gather(up_weight, "sp", axis=0, tiled=True),
        preferred_element_type=jnp.float32,
    )
    hidden = (jax.nn.silu(gate_part) * up_part).astype(jnp.bfloat16)
    partial_terms = jnp.dot(
        hidden,
        lax.all_gather(down_weight, "sp", axis=1, tiled=True),
        preferred_element_type=jnp.float32,
    )
    lowered = lax.psum_scatter(
        partial_terms.astype(jnp.bfloat16), "tp", scatter_dimension=0, tiled=True
    ).astype(jnp.float32)
    lowered = lax.optimization_barrier(lowered.astype(jnp.bfloat16)).astype(jnp.float32)
    result = layer_norm(ALPHA * normed.astype(jnp.float32) + lowered, ffn_gain, ffn_bias)
    return result.astype(jnp.bfloat16)


def solution(mesh):
    placed = (
        P("sp", "tp"),
        P("sp", "tp"),
        P("sp", "tp"),
        P("sp", "tp"),
        P("sp", None),
        P("tp", None),
        P(),
        P(),
        P("sp", "tp"),
        P("sp", "tp"),
        P("tp", "sp"),
        P(),
        P(),
    )
    return jax.shard_map(
        body, mesh=mesh, in_specs=placed, out_specs=P(("sp", "tp"), None), check_vma=False
    )
```

profile of v0, /device:TPU:0, one launch (start us, length us, event | category | flops | bytes accessed | tf_op | source)
XLA Modules:
  0.0 859.3 jit_solution(4486789846693739934)
XLA Ops:
  6.5 0.7 all-gather.7.cloned.1.call-update
  8.1 1.4 copy.18
  9.5 35.9 %all_gather.22 = f32[6144,8]{0,1:T(8,128)} all-gather(f32[768,8]{0,1:T(8,128)S(1)} %copy-done.6), channel_id=1, replica_groups=mesh['sp'=8,'tp'=4] {'sp'}, dimensions={0}, use_global_device_ids=true | all-gather | bytes 221184 | tf_op jit(solution)/shard_map/all_gather | solution.py:26
  45.4 66.8 %all-gather.7.cloned.1.call-done = bf16[6144,512]{1,0:T(8,128)(2,1)} async-done(((bf16[768,512]{1,0:T(8,128)(2,1)}), bf16[6144,512]{1,0:T(8,128)(2,1)}) %all-gather.7.cloned.1.call-update) | async-done | bytes 6291472 | tf_op jit(solution)/shard_map/all_gather | solution.py:33
  112.2 16.3 %reshape.82 = bf16[8,768,8,64]{3,2,1,0:T(8,128)(2,1)} reshape(bf16[6144,512]{1,0:T(8,128)(2,1)} %all-gather.7.cloned.1.call-done) | data formatting | bytes 12582912 | tf_op jit(solution)/shard_map/reshape | solution.py:46
  128.4 13.3 %copy.20 = bf16[8,768,8,64]{1,3,2,0:T(8,128)(2,1)} copy(bf16[8,768,8,64]{3,2,1,0:T(8,128)(2,1)} %reshape.82) | data formatting | bytes 12582912
  141.7 69.5 %all-gather.9.cloned.1.call-done = bf16[6144,512]{1,0:T(8,128)(2,1)} async-done(((bf16[768,512]{1,0:T(8,128)(2,1)}), bf16[6144,512]{1,0:T(8,128)(2,1)}) %all-gather.9.cloned.1.call-update) | async-done | bytes 6291472 | tf_op jit(solution)/shard_map/all_gather | solution.py:34
  211.2 16.2 %reshape.83 = bf16[8,768,8,64]{3,2,1,0:T(8,128)(2,1)} reshape(bf16[6144,512]{1,0:T(8,128)(2,1)} %all-gather.9.cloned.1.call-done) | data formatting | bytes 12582912 | tf_op jit(solution)/shard_map/reshape | solution.py:47
  227.5 13.2 %copy.21 = bf16[8,768,8,64]{1,3,2,0:T(8,128)(2,1)} copy(bf16[8,768,8,64]{3,2,1,0:T(8,128)(2,1)} %reshape.83) | data formatting | bytes 12582912
  240.6 1.3 broadcast_in_dim.52
  242.0 34.5 %while.15 = (s32[]{:T(128)}, f32[8,768]{1,0:T(8,128)S(1)}, f32[8,768]{1,0:T(8,128)S(1)}, f32[768,8,64]{0,2,1:T(8,128)}, s32[8]{0:T(128)S(1)}, /*index=5*/s32[]{:...) while((s32[]{:T(128)}, f32[8,768]{1,0:T(8,128)S(1)}, ...), condition=%wide.region_5.6_spmd.clone, body=%wide.region_0.5_spmd.clone.sunk | while | flops 1299009024 | bytes 77679992 | solution.py:83
  243.2 23.8 %conditional.3 = ((f32[8,768]{1,0:T(8,128)S(1)}, f32[8,768]{1,0:T(8,128)S(1)}, f32[768,8,64]{0,2,1:T(8,128)})) conditional(s32[]{:T(128)} %convert_element_type.96, (f32[8,768]{1,0:T(8,128)S(1)}, f32[8,768]{1,0:T(8,128)S(1)}, f32[768,8,64]{0,2,1:T(8,128)}) %tuple.40, (s32[]{:T(128)}, s32[]{:T(128)}, bf16[8,768,8,64]{1,3,2,0:T(8,128)(2,1)}, s32[]{:T(128)}, ...), branch_computations={%region_1.1_spmd, %region_2.4_spmd} | conditional | flops 1299009024 | bytes 77676648 | solution.py:81
  244.3 0.7 dynamic-slice_bitcast_fusion
  245.0 6.6 fusion.4
  251.7 8.0 bitcast_add_fusion
  259.7 7.3 fusion.3
  276.4 1.5 divide_convert_fusion
  278.0 3.5 convolution_convert_fusion
  282.2 202.4 %reduce-scatter.3.cloned.1.call-done = bf16[192,2048]{1,0:T(8,128)(2,1)} async-done(((bf16[768,2048]{1,0:T(8,128)(2,1)}), bf16[192,2048]{1,0:T(8,128)(2,1)}) %reduce-scatter.3.cloned.1.call-update) | async-done | bytes 786448 | tf_op jit(solution)/shard_map/reduce_scatter | solution.py:109
  484.6 1.8 fusion.21
  486.4 1.8 multiply_reduce_fusion.1
  488.2 2.5 add_convert_fusion.1
  492.1 86.8 %all-gather.13.cloned.1.call-done = bf16[2048,1408]{1,0:T(8,128)(2,1)} async-done(((bf16[256,1408]{1,0:T(8,128)(2,1)}), bf16[2048,1408]{1,0:T(8,128)(2,1)}) %all-gather.13.cloned.1.call-update) | async-done | bytes 5767184 | tf_op jit(solution)/shard_map/all_gather | solution.py:123
  579.0 28.1 %all-gather.11.cloned.1.call-done = bf16[768,2048]{1,0:T(8,128)(2,1)} async-done(((bf16[192,2048]{1,0:T(8,128)(2,1)}), bf16[768,2048]{1,0:T(8,128)(2,1)}) %all-gather.11.cloned.1.call-update) | async-done | bytes 3145744 | tf_op jit(solution)/shard_map/all_gather | solution.py:120
  607.1 9.7 %fusion.24 = f32[768,1408]{1,0:T(8,128)} fusion(bf16[768,2048]{1,0:T(8,128)(2,1)} %all-gather.11.cloned.1.call-done, bf16[2048,1408]{1,0:T(8,128)(2,1)} %all-gather.13.cloned.1.call-done), kind=kOutput, calls=%fused_computation.44 | convolution fusion | flops 4429185024 | bytes 13238272 | tf_op jit(solution)/shard_map/dot_general | solution.py:121
  616.8 84.7 %all-gather.15.cloned.1.call-done = bf16[2048,1408]{1,0:T(8,128)(2,1)} async-done(((bf16[256,1408]{1,0:T(8,128)(2,1)}), bf16[2048,1408]{1,0:T(8,128)(2,1)}) %all-gather.15.cloned.1.call-update) | async-done | bytes 5767184 | tf_op jit(solution)/shard_map/all_gather | solution.py:128
  701.5 93.4 %all-gather.17.cloned.1.call-done = bf16[1408,2048]{1,0:T(8,128)(2,1)} async-done(((bf16[1408,256]{1,0:T(8,128)(2,1)}), bf16[1408,2048]{1,0:T(8,128)(2,1)}) %all-gather.17.cloned.1.call-update) | async-done | bytes 5767184 | tf_op jit(solution)/shard_map/all_gather | solution.py:134
  794.9 16.8 %convolution_convert_fusion.1 = bf16[768,2048]{1,0:T(8,128)(2,1)} fusion(bf16[1408,2048]{1,0:T(8,128)(2,1)} %all-gather.17.cloned.1.call-done, f32[768,1408]{1,0:T(8,128)} %fusion.24, bf16[768,2048]{1,0:T(8,128)(2,1)} %all-gather.11.cloned.1.call-done, bf16[2048,1408]{1,0:T(8,128)(2,1)} %all-gather.15.cloned.1.call-done), kind=kOutput, calls=%fused_computation.28 | convolution fusion | flops 8866430976 | bytes 22151168 | tf_op jit(solution)/shard_map/dot_general | solution.py:132
  811.7 36.2 %reduce-scatter.5.cloned.1.call-done = bf16[192,2048]{1,0:T(8,128)(2,1)} async-done(((bf16[768,2048]{1,0:T(8,128)(2,1)}), bf16[192,2048]{1,0:T(8,128)(2,1)}) %reduce-scatter.5.cloned.1.call-update) | async-done | bytes 786448 | tf_op jit(solution)/shard_map/reduce_scatter | solution.py:137
  847.9 1.5 fusion.22
  849.5 1.6 multiply_reduce_fusion
  851.1 1.3 add_convert_fusion
  (72 shorter events, 9.1 us)
Async XLA Ops:
  6.5 271.4 %copy-start = (bf16[512,2048]{1,0:T(8,128)(2,1)S(1)}, bf16[512,2048]{1,0:T(8,128)(2,1)}, u32[]{:S(2)}) copy-start(bf16[512,2048]{1,0:T(8,128)(2,1)} %param.22) | copy-start | bytes 6291460
  6.5 2.9 copy-start.6
  6.5 105.6 %all-gather.7.cloned.1.call-start = ((), (), s32[]{:S(2)}) async-start(), calls=%async_computation.2 | async-start | bytes 7077888 | tf_op jit(solution)/shard_map/all_gather | solution.py:33
  7.3 204.0 %all-gather.9.cloned.1.call-start = ((), (), s32[]{:S(2)}) async-start(), calls=%async_computation.3 | async-start | bytes 7077888 | tf_op jit(solution)/shard_map/all_gather | solution.py:34
  8.0 476.6 %reduce-scatter.3.cloned.1.call-start = ((), (), s32[]{:S(2)}) async-start(), calls=%async_computation.4 | async-start | bytes 3932160 | tf_op jit(solution)/shard_map/reduce_scatter | solution.py:109
  245.0 6.6 copy-start.4
  259.7 7.4 copy-start.5
  281.5 206.7 %copy-start.7 = (f32[2048]{0:T(1024)S(1)}, f32[2048]{0:T(1024)}, u32[]{:S(2)}) copy-start(f32[2048]{0:T(1024)} %param.24) | copy-start | bytes 24580
  281.5 206.7 %copy-start.8 = (f32[2048]{0:T(1024)S(1)}, f32[2048]{0:T(1024)}, u32[]{:S(2)}) copy-start(f32[2048]{0:T(1024)} %param.23) | copy-start | bytes 24580
  281.6 297.4 %all-gather.13.cloned.1.call-start = ((), (), s32[]{:S(2)}) async-start(), calls=%async_computation.6 | async-start | bytes 6488064 | tf_op jit(solution)/shard_map/all_gather | solution.py:123
  282.1 325.0 %all-gather.11.cloned.1.call-start = ((), (), s32[]{:S(2)}) async-start(), calls=%async_computation.5 | async-start | bytes 3932160 | tf_op jit(solution)/shard_map/all_gather | solution.py:120
  484.6 3.6 copy-start.2
  490.8 210.7 %all-gather.15.cloned.1.call-start = ((), (), s32[]{:S(2)}) async-start(), calls=%async_computation.7 | async-start | bytes 6488064 | tf_op jit(solution)/shard_map/all_gather | solution.py:128
  491.3 303.5 %all-gather.17.cloned.1.call-start = ((), (), s32[]{:S(2)}) async-start(), calls=%async_computation.8 | async-start | bytes 6488064 | tf_op jit(solution)/shard_map/all_gather | solution.py:134
  492.1 355.8 %reduce-scatter.5.cloned.1.call-start = ((), (), s32[]{:S(2)}) async-start(), calls=%async_computation.9 | async-start | bytes 3932160 | tf_op jit(solution)/shard_map/reduce_scatter | solution.py:137
  811.6 36.3 %copy-start.1 = (bf16[192,2048]{1,0:T(8,128)(2,1)S(1)}, bf16[192,2048]{1,0:T(8,128)(2,1)}, u32[]{:S(2)}) copy-start(bf16[192,2048]{1,0:T(8,128)(2,1)} %add_convert_fusion.1) | copy-start | bytes 2359300
  811.6 39.4 %copy-start.9 = (f32[2048]{0:T(1024)S(1)}, f32[2048]{0:T(1024)}, u32[]{:S(2)}) copy-start(f32[2048]{0:T(1024)} %param.29) | copy-start | bytes 24580
  811.6 39.4 %copy-start.10 = (f32[2048]{0:T(1024)S(1)}, f32[2048]{0:T(1024)}, u32[]{:S(2)}) copy-start(f32[2048]{0:T(1024)} %param.28) | copy-start | bytes 24580
  847.9 3.2 copy-start.3
Sparse Core Ops, SparseCore 0:
  9.5 102.5 all-gather.6
  114.3 96.8 all-gather.8
  281.7 202.8 reduce-scatter.2
  486.6 92.2 all-gather.12
  580.4 26.6 all-gather.10
  609.1 92.3 all-gather.14
  703.5 91.2 all-gather.16
  811.8 36.0 reduce-scatter.4
where the time goes:
time: 862 us; the launch traced here: 859 us
  waiting for transfers between devices  671 us (78%)
  local copies, waits for them, and re-layouts  67.6 us (8%)
  matrix products  44.6 us (5%)
  blocking collectives  35.9 us (4%)
  other arithmetic  20.5 us (2%)
  between operations  13.6 us (2%)
    reduce_scatter x1, waiting for transfers between devices, body(): lax.psum_scatter(jnp.dot(attended, out_weight, preferred_element_type=jnp...  202 us
    all_gather x1, waiting for transfers between devices, body(): lax.all_gather(down_weight, 'sp', axis=1, tiled=True)  93.4 us
    all_gather x1, waiting for transfers between devices, body(): lax.all_gather(gate_weight, 'sp', axis=0, tiled=True)  86.8 us
    all_gather x1, waiting for transfers between devices, body(): lax.all_gather(up_weight, 'sp', axis=0, tiled=True)  84.7 us
    all_gather x1, waiting for transfers between devices, attend(): value_piece = lax.all_gather(value_rows, 'sp', axis=0, tiled=True)  69.5 us
    all_gather x1, waiting for transfers between devices, attend(): key_piece = lax.all_gather(key_rows, 'sp', axis=0, tiled=True)  66.8 us
    reduce_scatter x1, waiting for transfers between devices, body(): lax.psum_scatter(partial_terms.astype(jnp.bfloat16), 'tp', scatter_dimens...  36.2 us
    all_gather x1, blocking collectives, attend(): gates_all = lax.all_gather(log_forget, 'sp', axis=0, tiled=True)  35.9 us
  transfers between devices with their start and end apart: 8, of which 8 were waited for; matrix products, arithmetic and copies ran while one was open for 5% of the time, Pallas kernels for 0%

commit v1 on v0

--- a/solution.py
+++ b/solution.py
@@ -31,7 +31,13 @@
     )
     running = initial
     key_piece = lax.all_gather(key_rows, "sp", axis=0, tiled=True)
-    value_piece = lax.all_gather(value_rows, "sp", axis=0, tiled=True)
+    size = lax.axis_size("sp")
+    moving, pieces = (value_rows, [value_rows])
+    for _ in range(size - 1):
+        moving = lax.ppermute(moving, "sp", [(i, (i + 1) % size) for i in range(size)])
+        pieces.insert(0, moving)
+    line = jnp.concatenate(pieces, axis=0)
+    value_piece = jnp.roll(line, (lax.axis_index("sp") + 1) * value_rows.shape[0], axis=0)
     piece_len = key_piece.shape[0]
     shards = piece_len // length
     group_size = max(

time: 862 us -> 940 us (1.090)
  waiting for transfers between devices: 671 us -> 718 us
  local copies, waits for them, and re-layouts: 67.6 us -> 84.5 us
    ppermute x0 -> x7, waiting for transfers between devices: none -> 186 us  [attend(): lax.ppermute(moving, 'sp', [(i, (i + 1) % size) for i in range(size)])]
    all_gather x1 -> x0, waiting for transfers between devices: 69.5 us -> none  [attend(): value_piece = lax.all_gather(value_rows, 'sp', axis=0, tiled=True)]
    all_gather x1, waiting for transfers between devices: 66.8 us -> 0.01 us  [attend(): key_piece = lax.all_gather(key_rows, 'sp', axis=0, tiled=True)]
    unnamed x21 -> x56, local copies, waits for them, and re-layouts: 27.9 us -> 40.9 us
  transfers between devices with their start and end apart: 8 -> 14, of which waited for: 8 -> 12; matrix products, arithmetic and copies ran while one was open for 5% -> 6% of each run, Pallas kernels for 0% -> 0%
where the time goes in v1:
time: 940 us; the launch traced here: 937 us
  waiting for transfers between devices  718 us (76%)
  local copies, waits for them, and re-layouts  84.5 us (9%)
  matrix products  44.6 us (5%)
  blocking collectives  44.3 us (5%)
  other arithmetic  21.7 us (2%)
  between operations  13.8 us (1%)
    reduce_scatter x1, waiting for transfers between devices, body(): lax.psum_scatter(jnp.dot(attended, out_weight, preferred_element_type=jnp...  200 us
    ppermute x7, waiting for transfers between devices, attend(): lax.ppermute(moving, 'sp', [(i, (i + 1) % size) for i in range(size)])  186 us
    all_gather x1, waiting for transfers between devices, body(): lax.all_gather(down_weight, 'sp', axis=1, tiled=True)  93.2 us
    all_gather x1, waiting for transfers between devices, body(): lax.all_gather(gate_weight, 'sp', axis=0, tiled=True)  87 us
    all_gather x1, waiting for transfers between devices, body(): lax.all_gather(up_weight, 'sp', axis=0, tiled=True)  84.7 us
    all_gather x1, blocking collectives, attend(): gates_all = lax.all_gather(log_forget, 'sp', axis=0, tiled=True)  44.3 us
    unnamed x56, local copies, waits for them, and re-layouts  40.9 us
    reduce_scatter x1, waiting for transfers between devices, body(): lax.psum_scatter(partial_terms.astype(jnp.bfloat16), 'tp', scatter_dimens...  36.2 us
  transfers between devices with their start and end apart: 14, of which 12 were waited for; matrix products, arithmetic and copies ran while one was open for 6% of the time, Pallas kernels for 0%

profile of v1, /device:TPU:0, one launch (start us, length us, event | category | flops | bytes accessed | tf_op | source)
XLA Modules:
  0.0 936.9 jit_solution(813044454784271184)
XLA Ops:
  7.3 3.0 collective-permute-start
  10.4 26.5 %collective-permute-done = bf16[768,512]{1,0:T(8,128)(2,1)S(1)} collective-permute-done((bf16[768,512]{1,0:T(8,128)(2,1)}, bf16[768,512]{1,0:T(8,128)(2,1)S(1)}, u32[]{:S(2)}, u32[]{:S(2)}) %collective-permute-start) | collective-permute-done | bytes 786464 | tf_op jit(solution)/shard_map/ppermute | solution.py:37
  38.3 35.1 %collective-permute-done.1 = bf16[768,512]{1,0:T(8,128)(2,1)S(1)} collective-permute-done((bf16[768,512]{1,0:T(8,128)(2,1)S(1)}, bf16[768,512]{1,0:T(8,128)(2,1)S(1)}, u32[]{:S(2)}, u32[]{:S(2)}) %collective-permute-start.1) | collective-permute-done | bytes 786464 | tf_op jit(solution)/shard_map/ppermute | solution.py:37
  74.3 38.9 %collective-permute-done.2 = bf16[768,512]{1,0:T(8,128)(2,1)S(1)} collective-permute-done((bf16[768,512]{1,0:T(8,128)(2,1)S(1)}, bf16[768,512]{1,0:T(8,128)(2,1)S(1)}, u32[]{:S(2)}, u32[]{:S(2)}) %collective-permute-start.2) | collective-permute-done | bytes 786464 | tf_op jit(solution)/shard_map/ppermute | solution.py:37
  114.1 38.7 %collective-permute-done.3 = bf16[768,512]{1,0:T(8,128)(2,1)S(1)} collective-permute-done((bf16[768,512]{1,0:T(8,128)(2,1)S(1)}, bf16[768,512]{1,0:T(8,128)(2,1)S(1)}, u32[]{:S(2)}, u32[]{:S(2)}) %collective-permute-start.3) | collective-permute-done | bytes 786464 | tf_op jit(solution)/shard_map/ppermute | solution.py:37
  153.7 26.2 %collective-permute-done.4 = bf16[768,512]{1,0:T(8,128)(2,1)S(1)} collective-permute-done((bf16[768,512]{1,0:T(8,128)(2,1)S(1)}, bf16[768,512]{1,0:T(8,128)(2,1)S(1)}, u32[]{:S(2)}, u32[]{:S(2)}) %collective-permute-start.4) | collective-permute-done | bytes 786464 | tf_op jit(solution)/shard_map/ppermute | solution.py:37
  180.8 20.9 %collective-permute-done.5 = bf16[768,512]{1,0:T(8,128)(2,1)} collective-permute-done((bf16[768,512]{1,0:T(8,128)(2,1)S(1)}, bf16[768,512]{1,0:T(8,128)(2,1)}, u32[]{:S(2)}, u32[]{:S(2)}) %collective-permute-start.5) | collective-permute-done | bytes 786464 | tf_op jit(solution)/shard_map/ppermute | solution.py:37
  201.7 2.3 copy.18
  204.0 44.3 %all_gather.19 = f32[6144,8]{0,1:T(8,128)} all-gather(f32[768,8]{0,1:T(8,128)} %param.20), channel_id=1, replica_groups=mesh['sp'=8,'tp'=4] {'sp'}, dimensions={0}, use_global_device_ids=true | all-gather | bytes 221184 | tf_op jit(solution)/shard_map/all_gather | solution.py:26
  256.2 4.2 constant_dynamic-slice_fusion
  260.4 16.2 %reshape.83 = bf16[8,768,8,64]{3,2,1,0:T(8,128)(2,1)} reshape(bf16[6144,512]{1,0:T(8,128)(2,1)} %constant_dynamic-slice_fusion) | data formatting | bytes 12582912 | tf_op jit(solution)/shard_map/reshape | solution.py:53
  276.6 13.1 %copy.21 = bf16[8,768,8,64]{1,3,2,0:T(8,128)(2,1)} copy(bf16[8,768,8,64]{3,2,1,0:T(8,128)(2,1)} %reshape.83) | data formatting | bytes 12582912
  289.8 16.2 %reshape.82 = bf16[8,768,8,64]{3,2,1,0:T(8,128)(2,1)} reshape(bf16[6144,512]{1,0:T(8,128)(2,1)} %all-gather.6.cloned.1.call-done) | data formatting | bytes 12582912 | tf_op jit(solution)/shard_map/reshape | solution.py:52
  306.0 13.3 %copy.20 = bf16[8,768,8,64]{1,3,2,0:T(8,128)(2,1)} copy(bf16[8,768,8,64]{3,2,1,0:T(8,128)(2,1)} %reshape.82) | data formatting | bytes 12582912
  320.6 34.5 %while.15 = (s32[]{:T(128)}, f32[8,768]{1,0:T(8,128)S(1)}, f32[8,768]{1,0:T(8,128)S(1)}, f32[768,8,64]{0,2,1:T(8,128)}, s32[8]{0:T(128)S(1)}, /*index=5*/s32[]{:...) while((s32[]{:T(128)}, f32[8,768]{1,0:T(8,128)S(1)}, ...), condition=%wide.region_5.6_spmd.clone, body=%wide.region_0.5_spmd.clone.sunk | while | flops 1299009024 | bytes 77679992 | solution.py:89
  322.0 23.9 %conditional.3 = ((f32[8,768]{1,0:T(8,128)S(1)}, f32[8,768]{1,0:T(8,128)S(1)}, f32[768,8,64]{0,2,1:T(8,128)})) conditional(s32[]{:T(128)} %convert_element_type.96, (f32[8,768]{1,0:T(8,128)S(1)}, f32[8,768]{1,0:T(8,128)S(1)}, f32[768,8,64]{0,2,1:T(8,128)}) %tuple.40, (s32[]{:T(128)}, s32[]{:T(128)}, bf16[8,768,8,64]{1,3,2,0:T(8,128)(2,1)}, s32[]{:T(128)}, ...), branch_computations={%region_1.1_spmd, %region_2.4_spmd} | conditional | flops 1299009024 | bytes 77676648 | solution.py:87
  323.9 6.6 fusion.4
  330.5 8.0 bitcast_add_fusion
  338.5 7.3 fusion.3
  356.7 3.5 convolution_convert_fusion
  361.0 200.2 %reduce-scatter.3.cloned.1.call-done = bf16[192,2048]{1,0:T(8,128)(2,1)} async-done(((bf16[768,2048]{1,0:T(8,128)(2,1)}), bf16[192,2048]{1,0:T(8,128)(2,1)}) %reduce-scatter.3.cloned.1.call-update) | async-done | bytes 786448 | tf_op jit(solution)/shard_map/reduce_scatter | solution.py:115
  561.2 1.7 fusion.21
  562.9 1.8 multiply_reduce_fusion.1
  564.8 2.7 add_convert_fusion.1
  568.7 87.0 %all-gather.10.cloned.1.call-done = bf16[2048,1408]{1,0:T(8,128)(2,1)} async-done(((bf16[256,1408]{1,0:T(8,128)(2,1)}), bf16[2048,1408]{1,0:T(8,128)(2,1)}) %all-gather.10.cloned.1.call-update) | async-done | bytes 5767184 | tf_op jit(solution)/shard_map/all_gather | solution.py:129
  655.8 28.1 %all-gather.8.cloned.1.call-done = bf16[768,2048]{1,0:T(8,128)(2,1)} async-done(((bf16[192,2048]{1,0:T(8,128)(2,1)}), bf16[768,2048]{1,0:T(8,128)(2,1)}) %all-gather.8.cloned.1.call-update) | async-done | bytes 3145744 | tf_op jit(solution)/shard_map/all_gather | solution.py:126
  683.9 9.7 %fusion.24 = f32[768,1408]{1,0:T(8,128)} fusion(bf16[768,2048]{1,0:T(8,128)(2,1)} %all-gather.8.cloned.1.call-done, bf16[2048,1408]{1,0:T(8,128)(2,1)} %all-gather.10.cloned.1.call-done), kind=kOutput, calls=%fused_computation.61 | convolution fusion | flops 4429185024 | bytes 13238272 | tf_op jit(solution)/shard_map/dot_general | solution.py:127
  693.6 84.7 %all-gather.12.cloned.1.call-done = bf16[2048,1408]{1,0:T(8,128)(2,1)} async-done(((bf16[256,1408]{1,0:T(8,128)(2,1)}), bf16[2048,1408]{1,0:T(8,128)(2,1)}) %all-gather.12.cloned.1.call-update) | async-done | bytes 5767184 | tf_op jit(solution)/shard_map/all_gather | solution.py:134
  778.3 93.2 %all-gather.14.cloned.1.call-done = bf16[1408,2048]{1,0:T(8,128)(2,1)} async-done(((bf16[1408,256]{1,0:T(8,128)(2,1)}), bf16[1408,2048]{1,0:T(8,128)(2,1)}) %all-gather.14.cloned.1.call-update) | async-done | bytes 5767184 | tf_op jit(solution)/shard_map/all_gather | solution.py:140
  871.5 16.8 %convolution_convert_fusion.1 = bf16[768,2048]{1,0:T(8,128)(2,1)} fusion(bf16[1408,2048]{1,0:T(8,128)(2,1)} %all-gather.14.cloned.1.call-done, f32[768,1408]{1,0:T(8,128)} %fusion.24, bf16[768,2048]{1,0:T(8,128)(2,1)} %all-gather.8.cloned.1.call-done, bf16[2048,1408]{1,0:T(8,128)(2,1)} %all-gather.12.cloned.1.call-done), kind=kOutput, calls=%fused_computation.28 | convolution fusion | flops 8866430976 | bytes 22151168 | tf_op jit(solution)/shard_map/dot_general | solution.py:138
  888.3 36.2 %reduce-scatter.5.cloned.1.call-done = bf16[192,2048]{1,0:T(8,128)(2,1)} async-done(((bf16[768,2048]{1,0:T(8,128)(2,1)}), bf16[192,2048]{1,0:T(8,128)(2,1)}) %reduce-scatter.5.cloned.1.call-update) | async-done | bytes 786448 | tf_op jit(solution)/shard_map/reduce_scatter | solution.py:143
  927.6 2.5 add_convert_fusion
  (120 shorter events, 28.1 us)
Async XLA Ops:
  6.5 350.1 %copy-start = (bf16[512,2048]{1,0:T(8,128)(2,1)S(1)}, bf16[512,2048]{1,0:T(8,128)(2,1)}, u32[]{:S(2)}) copy-start(bf16[512,2048]{1,0:T(8,128)(2,1)} %param.22) | copy-start | bytes 6291460
  6.5 283.2 %all-gather.6.cloned.1.call-start = ((), (), s32[]{:S(2)}) async-start(), calls=%async_computation.2 | async-start | bytes 7077888 | tf_op jit(solution)/shard_map/all_gather | solution.py:33
  7.3 554.0 %reduce-scatter.3.cloned.1.call-start = ((), (), s32[]{:S(2)}) async-start(), calls=%async_computation.3 | async-start | bytes 3932160 | tf_op jit(solution)/shard_map/reduce_scatter | solution.py:115
  7.3 29.6 %collective-permute-start = (bf16[768,512]{1,0:T(8,128)(2,1)}, bf16[768,512]{1,0:T(8,128)(2,1)S(1)}, u32[]{:S(2)}, u32[]{:S(2)}) collective-permute-start(bf16[768,512]{1,0:T(8,128)(2,1)} %param.19), channel_id=1, source_target_pairs={{0,4},{4,8},{8,12},{12,16},{16,20},{20,24},{24,28},{28,0},{1,5},{5... | collective-permute-start | bytes 2359304 | tf_op jit(solution)/shard_map/ppermute | solution.py:37
  36.9 0.9 copy-start.5
  37.8 35.6 %collective-permute-start.1 = (bf16[768,512]{1,0:T(8,128)(2,1)S(1)}, bf16[768,512]{1,0:T(8,128)(2,1)S(1)}, u32[]{:S(2)}, u32[]{:S(2)}) collective-permute-start(bf16[768,512]{1,0:T(8,128)(2,1)S(1)} %collective-permute-done), channel_id=1, source_target_pairs={{0,4},{4,8},{8,12},{12,16},{16,20},{20,24},{24,28},{28,0},{1,5},{5... | collective-permute-start | bytes 2359304 | tf_op jit(solution)/shard_map/ppermute | solution.py:37
  74.3 38.9 %collective-permute-start.2 = (bf16[768,512]{1,0:T(8,128)(2,1)S(1)}, bf16[768,512]{1,0:T(8,128)(2,1)S(1)}, u32[]{:S(2)}, u32[]{:S(2)}) collective-permute-start(bf16[768,512]{1,0:T(8,128)(2,1)S(1)} %collective-permute-done.1), channel_id=1, source_target_pairs={{0,4},{4,8},{8,12},{12,16},{16,20},{20,24},{24,28},{28,0},{1,5},{5... | collective-permute-start | bytes 2359304 | tf_op jit(solution)/shard_map/ppermute | solution.py:37
  114.1 38.7 %collective-permute-start.3 = (bf16[768,512]{1,0:T(8,128)(2,1)S(1)}, bf16[768,512]{1,0:T(8,128)(2,1)S(1)}, u32[]{:S(2)}, u32[]{:S(2)}) collective-permute-start(bf16[768,512]{1,0:T(8,128)(2,1)S(1)} %collective-permute-done.2), channel_id=1, source_target_pairs={{0,4},{4,8},{8,12},{12,16},{16,20},{20,24},{24,28},{28,0},{1,5},{5... | collective-permute-start | bytes 2359304 | tf_op jit(solution)/shard_map/ppermute | solution.py:37
  153.7 26.2 %collective-permute-start.4 = (bf16[768,512]{1,0:T(8,128)(2,1)S(1)}, bf16[768,512]{1,0:T(8,128)(2,1)S(1)}, u32[]{:S(2)}, u32[]{:S(2)}) collective-permute-start(bf16[768,512]{1,0:T(8,128)(2,1)S(1)} %collective-permute-done.3), channel_id=1, source_target_pairs={{0,4},{4,8},{8,12},{12,16},{16,20},{20,24},{24,28},{28,0},{1,5},{5... | collective-permute-start | bytes 2359304 | tf_op jit(solution)/shard_map/ppermute | solution.py:37
  179.9 0.9 copy-start.13
  180.8 20.9 %collective-permute-start.5 = (bf16[768,512]{1,0:T(8,128)(2,1)S(1)}, bf16[768,512]{1,0:T(8,128)(2,1)}, u32[]{:S(2)}, u32[]{:S(2)}) collective-permute-start(bf16[768,512]{1,0:T(8,128)(2,1)S(1)} %collective-permute-done.4), channel_id=1, source_target_pairs={{0,4},{4,8},{8,12},{12,16},{16,20},{20,24},{24,28},{28,0},{1,5},{5... | collective-permute-start | bytes 2359304 | tf_op jit(solution)/shard_map/ppermute | solution.py:37
  201.7 46.6 %collective-permute-start.6 = (bf16[768,512]{1,0:T(8,128)(2,1)}, bf16[768,512]{1,0:T(8,128)(2,1)}, u32[]{:S(2)}, u32[]{:S(2)}) collective-permute-start(bf16[768,512]{1,0:T(8,128)(2,1)} %collective-permute-done.5), channel_id=1, source_target_pairs={{0,4},{4,8},{8,12},{12,16},{16,20},{20,24},{24,28},{28,0},{1,5},{5... | collective-permute-start | bytes 2359304 | tf_op jit(solution)/shard_map/ppermute | solution.py:37
  204.0 49.4 %copy-start.4 = (bf16[768,512]{1,0:T(8,128)(2,1)S(1)}, bf16[768,512]{1,0:T(8,128)(2,1)}, u32[]{:S(2)}) copy-start(bf16[768,512]{1,0:T(8,128)(2,1)} %param.19) | copy-start | bytes 2359300
  204.0 49.1 %copy-start.10 = (bf16[768,512]{1,0:T(8,128)(2,1)S(1)}, bf16[768,512]{1,0:T(8,128)(2,1)}, u32[]{:S(2)}) copy-start(bf16[768,512]{1,0:T(8,128)(2,1)} %copy-done.9) | copy-start | bytes 2359300
  204.0 49.2 %copy-start.8 = (bf16[768,512]{1,0:T(8,128)(2,1)S(1)}, bf16[768,512]{1,0:T(8,128)(2,1)}, u32[]{:S(2)}) copy-start(bf16[768,512]{1,0:T(8,128)(2,1)} %copy-done.7) | copy-start | bytes 2359300
  204.0 49.3 %copy-start.6 = (bf16[768,512]{1,0:T(8,128)(2,1)S(1)}, bf16[768,512]{1,0:T(8,128)(2,1)}, u32[]{:S(2)}) copy-start(bf16[768,512]{1,0:T(8,128)(2,1)} %copy-done.5) | copy-start | bytes 2359300
  251.8 3.9 copy-start.14
  253.1 2.7 copy-start.12
  306.0 14.6 %copy-start.15 = (f32[768,8]{0,1:T(8,128)S(1)}, f32[768,8]{0,1:T(8,128)}, u32[]{:S(2)}) copy-start(f32[768,8]{0,1:T(8,128)} %param.20) | copy-start | bytes 73732
  306.0 14.6 %copy-start.16 = (bf16[768,512]{0,1:T(8,128)(2,1)S(1)}, bf16[768,512]{0,1:T(8,128)(2,1)}, u32[]{:S(2)}) copy-start(bf16[768,512]{0,1:T(8,128)(2,1)} %copy.18) | copy-start | bytes 2359300
  323.9 6.6 copy-start.2
  338.5 7.4 copy-start.3
  356.6 208.1 %copy-start.17 = (f32[2048]{0:T(1024)S(1)}, f32[2048]{0:T(1024)}, u32[]{:S(2)}) copy-start(f32[2048]{0:T(1024)} %param.24) | copy-start | bytes 24580
  356.7 208.1 %copy-start.18 = (f32[2048]{0:T(1024)S(1)}, f32[2048]{0:T(1024)}, u32[]{:S(2)}) copy-start(f32[2048]{0:T(1024)} %param.23) | copy-start | bytes 24580
  360.2 295.5 %all-gather.10.cloned.1.call-start = ((), (), s32[]{:S(2)}) async-start(), calls=%async_computation.5 | async-start | bytes 6488064 | tf_op jit(solution)/shard_map/all_gather | solution.py:129
  361.0 322.9 %all-gather.8.cloned.1.call-start = ((), (), s32[]{:S(2)}) async-start(), calls=%async_computation.4 | async-start | bytes 3932160 | tf_op jit(solution)/shard_map/all_gather | solution.py:126
  567.5 210.7 %all-gather.12.cloned.1.call-start = ((), (), s32[]{:S(2)}) async-start(), calls=%async_computation.6 | async-start | bytes 6488064 | tf_op jit(solution)/shard_map/all_gather | solution.py:134
  568.1 303.4 %all-gather.14.cloned.1.call-start = ((), (), s32[]{:S(2)}) async-start(), calls=%async_computation.7 | async-start | bytes 6488064 | tf_op jit(solution)/shard_map/all_gather | solution.py:140
  568.7 355.8 %reduce-scatter.5.cloned.1.call-start = ((), (), s32[]{:S(2)}) async-start(), calls=%async_computation.8 | async-start | bytes 3932160 | tf_op jit(solution)/shard_map/reduce_scatter | solution.py:143
  693.6 231.0 %copy-start.1 = (bf16[192,2048]{1,0:T(8,128)(2,1)S(1)}, bf16[192,2048]{1,0:T(8,128)(2,1)}, u32[]{:S(2)}) copy-start(bf16[192,2048]{1,0:T(8,128)(2,1)} %add_convert_fusion.1) | copy-start | bytes 2359300
  888.3 39.3 %copy-start.19 = (f32[2048]{0:T(1024)S(1)}, f32[2048]{0:T(1024)}, u32[]{:S(2)}) copy-start(f32[2048]{0:T(1024)} %param.29) | copy-start | bytes 24580
  888.3 39.3 %copy-start.20 = (f32[2048]{0:T(1024)S(1)}, f32[2048]{0:T(1024)}, u32[]{:S(2)}) copy-start(f32[2048]{0:T(1024)} %param.28) | copy-start | bytes 24580
  (3 other events, 2.7 us)
Sparse Core Ops, SparseCore 0:
  9.5 146.4 all-gather.5
  360.3 200.8 reduce-scatter.2
  563.4 92.2 all-gather.9
  657.2 26.6 all-gather.7
  685.9 92.3 all-gather.11
  780.2 91.2 all-gather.13
  888.4 36.0 reduce-scatter.4
